TPU v7x, 256 devices: a whole 4x4x8 slice. The times are simulated.
256 devices in a mesh: row: 32 (over z, y), col: 8 (over x, core).
Axes of the slice: x: 4, y: 4, z: 8, core: 2. Of those that a mesh axis runs over, the one named last changes fastest.
Arguments:
- tokens: bfloat16 [2, 65536, 1024], P(None, 'row'), may hold values from -6 to 6
- norm_gain: float32 [1024], replicated, may hold values from 0.1 to 1.9
- w_fourier_in: bfloat16 [1024, 512], P(None, 'col'), may hold values from -0.1875 to 0.1875
- w_gate: bfloat16 [1024, 1024], replicated, may hold values from -0.1875 to 0.1875
- w_spectrum: bfloat16 [512, 1024], replicated, may hold values from -0.25 to 0.25
- w_output: bfloat16 [1024, 1024], P(None, 'col'), may hold values from -0.375 to 0.375
Outputs:
- block_output: bfloat16 [2, 65536, 1024], P(None, 'row', 'col')
All inputs are finite; a program needn't handle non-finite values.
Results may differ from a plain program's by a relative error of at most 0.015.
Values may be sent and summed in bfloat16 or wider, within the bound.
A program may use at most 320 MiB of HBM per device.

v0:
```python
import jax
import jax.numpy as jnp
from jax import lax
from jax.sharding import PartitionSpec as P

GROUP_WIDTH = 64
FIRST_LEN = 256


norm_eps = 1e-06


def shortened(value):
    return jax.tree.map(lambda a: a.astype(jnp.bfloat16) if a.dtype == jnp.float32 else a, value)


def over_all(value, axis, dim, absorb, carry):
    whole = jax.tree.map(lambda part: lax.all_gather(part, axis, axis=dim, tiled=True), value)
    return absorb(carry, whole, jnp.int32(0))


def dft_tables(length_in, length_out, period):
    left_index = lax.broadcasted_iota(jnp.int32, (length_in, length_out), 0)
    right_index = lax.broadcasted_iota(jnp.int32, (length_in, length_out), 1)
    angles = (left_index * right_index % period).astype(jnp.float32) * (2.0 * jnp.pi / period)
    return (jnp.cos(angles), jnp.sin(angles))


def transform_first(cube, table):
    return jnp.einsum("cpq,pk->ckq", cube, table, precision=lax.Precision.HIGHEST)


def transform_second(cube, table):
    return jnp.einsum("ckq,qj->cjk", cube, table, precision=lax.Precision.HIGHEST)


def positional(real_part, imag_part):
    rows_count, seq_total = real_part.shape
    second_len = seq_total // FIRST_LEN
    cos_first, sin_first = dft_tables(FIRST_LEN, FIRST_LEN, FIRST_LEN)
    cos_twist, sin_twist = dft_tables(FIRST_LEN, second_len, seq_total)
    cos_second, sin_second = dft_tables(second_len, second_len, second_len)
    real_cube = real_part.reshape(rows_count, FIRST_LEN, second_len)
    imag_cube = imag_part.reshape(rows_count, FIRST_LEN, second_len)
    section_real = transform_first(real_cube, cos_first) + transform_first(imag_cube, sin_first)
    section_imag = transform_first(imag_cube, cos_first) - transform_first(real_cube, sin_first)
    twist_real = section_real * cos_twist + section_imag * sin_twist
    twist_imag = section_imag * cos_twist - section_real * sin_twist
    summed = transform_second(twist_real, cos_second) + transform_second(twist_imag, sin_second)
    norm_scale = 1.0 / jnp.sqrt(jnp.float32(seq_total * GROUP_WIDTH))
    return (summed.reshape(rows_count, seq_total) * norm_scale).astype(jnp.bfloat16)


def on_device(tokens, norm_gain, w_fourier_in, w_gate, w_spectrum, w_output):
    batches, seq_local, features = tokens.shape
    tokens_count = batches * seq_local
    widened = tokens.astype(jnp.float32)
    inverse = lax.rsqrt(jnp.mean(widened * widened, axis=-1, keepdims=True) + norm_eps)
    normed = (widened * inverse * norm_gain).astype(jnp.bfloat16).reshape(tokens_count, features)
    fourier_in = jnp.dot(normed, w_fourier_in, preferred_element_type=jnp.float32).astype(
        jnp.bfloat16
    )
    local_groups = w_fourier_in.shape[1] // GROUP_WIDTH
    grouped = fourier_in.astype(jnp.float32).reshape(batches, seq_local, local_groups, GROUP_WIDTH)
    cos_group, sin_group = dft_tables(GROUP_WIDTH, GROUP_WIDTH, GROUP_WIDTH)
    real_part = jnp.einsum(
        "btgn,nm->bgmt", grouped, cos_group, precision=lax.Precision.HIGHEST
    ).reshape(-1, seq_local)
    imag_part = -jnp.einsum(
        "btgn,nm->bgmt", grouped, sin_group, precision=lax.Precision.HIGHEST
    ).reshape(-1, seq_local)
    real_part = lax.all_to_all(
        shortened(real_part), "row", split_axis=0, concat_axis=1, tiled=True
    ).astype(real_part.dtype)
    imag_part = lax.all_to_all(
        shortened(imag_part), "row", split_axis=0, concat_axis=1, tiled=True
    ).astype(imag_part.dtype)
    spectrum = positional(real_part, imag_part)
    spectrum = lax.all_to_all(spectrum, "row", split_axis=1, concat_axis=0, tiled=True)
    spectrum = spectrum.reshape(batches, local_groups * GROUP_WIDTH, seq_local)
    spectrum = jnp.transpose(spectrum, (0, 2, 1)).reshape(tokens_count, local_groups * GROUP_WIDTH)

    def add_spectrum(running, portion, beginning):
        weight_rows = lax.dynamic_slice_in_dim(w_spectrum, beginning, portion.shape[1], 0)
        return running + jnp.dot(portion, weight_rows, preferred_element_type=jnp.float32)

    mixed_pre = over_all(
        spectrum, "col", 1, add_spectrum, jnp.zeros((tokens_count, features), jnp.float32)
    ).astype(jnp.bfloat16)
    gate_pre = jnp.dot(normed, w_gate, preferred_element_type=jnp.float32)
    mixed = (jax.nn.sigmoid(gate_pre) * mixed_pre.astype(jnp.float32)).astype(jnp.bfloat16)
    result = jnp.dot(mixed, w_output, preferred_element_type=jnp.float32)
    return result.astype(jnp.bfloat16).reshape(batches, seq_local, -1)


def solution(mesh):
    placed = (P(None, "row", None), P(), P(None, "col"), P(), P(), P(None, "col"))
    return jax.shard_map(
        on_device, mesh=mesh, in_specs=placed, out_specs=P(None, "row", "col"), check_vma=False
    )
```

profile of v0, /device:TPU:1, one launch (start us, length us, event | category | flops | bytes accessed | tf_op | source)
XLA Modules:
  0.0 175.4 jit_solution(16493660522271949661)
XLA Ops:
  6.5 5.2 %fusion = f32[2,2048]{1,0:T(2,128)S(1)} fusion(bf16[2,2048,1024]{2,1,0:T(8,128)(2,1)} %param.6), kind=kLoop, calls=%fused_computation.2 | loop fusion | flops 12578816 | bytes 8404992 | tf_op jit(solution)/shard_map/reduce_sum | solution.py:58
  12.5 2.2 %fusion.2 = bf16[2,2048,1024]{2,1,0:T(8,128)(2,1)S(1)} fusion(bf16[2,2048,1024]{2,1,0:T(8,128)(2,1)S(1)} %copy-done.2, f32[1024]{0:T(1024)S(1)} %copy-done.5, f32[2,2048]{1,0:T(2,128)S(1)} %add_rsqrt_fusion), kind=kLoop, calls=%fused_computation.4 | loop fusion | flops 16777216 | bytes 16797696 | tf_op jit(solution)/shard_map/convert_element_type | solution.py:59
  14.7 3.2 %copy-done.1 = bf16[2,2048,1024]{2,1,0:T(8,128)(2,1)} copy-done((bf16[2,2048,1024]{2,1,0:T(8,128)(2,1)}, bf16[2,2048,1024]{2,1,0:T(8,128)(2,1)S(1)}, u32[]{:S(2)}) %copy-start.1) | copy-done | bytes 8388632
  17.9 2.7 %convolution_convert_fusion = bf16[4096,64]{0,1:T(8,128)(2,1)S(1)} fusion(bf16[4096,1024]{1,0:T(8,128)(2,1)S(1)} %bitcast.69, bf16[1024,64]{0,1:T(8,128)(2,1)S(1)} %copy-done.4), kind=kOutput, calls=%fused_computation.8 | convolution fusion | flops 537133056 | bytes 9043968 | tf_op jit(solution)/shard_map/dot_general | solution.py:60
  21.2 1.0 convert_element_type.107
  22.2 12.0 %all-to-all-start.1 = ((bf16[32,4,2048]{2,1,0:T(4,128)(2,1)}), bf16[32,4,2048]{2,1,0:T(4,128)(2,1)S(1)}, u32[]{:S(2)}, u32[]{:S(2)}) async-start(bf16[32,4,2048]{2,1,0:T(4,128)(2,1)} %convert_element_type.107), calls=%async_computation.1 | async-start | bytes 1048576 | tf_op jit(solution)/shard_map/all_to_all | solution.py:75
  34.3 1.5 fusion.6
  35.8 2.1 %convert_element_type.103 = bf16[32,4,2048]{2,1,0:T(4,128)(2,1)} reshape(bf16[2,1,64,2048]{3,2,0,1:T(8,128)(2,1)} %fusion.6) | data formatting | bytes 1048576 | tf_op jit(solution)/shard_map/convert_element_type | solution.py:14
  37.9 12.5 %all-to-all-done.1 = bf16[32,4,2048]{2,1,0:T(4,128)(2,1)S(1)} async-done(((bf16[32,4,2048]{2,1,0:T(4,128)(2,1)}), bf16[32,4,2048]{2,1,0:T(4,128)(2,1)S(1)}, u32[]{:S(2)}, u32[]{:S(2)}) %all-to-all-start.1) | async-done | bytes 524320 | tf_op jit(solution)/shard_map/all_to_all | solution.py:75
  50.3 5.7 %all-to-all-start = ((bf16[32,4,2048]{2,1,0:T(4,128)(2,1)}), bf16[32,4,2048]{2,1,0:T(4,128)(2,1)}, u32[]{:S(2)}, u32[]{:S(2)}) async-start(bf16[32,4,2048]{2,1,0:T(4,128)(2,1)} %convert_element_type.103), calls=%async_computation | async-start | bytes 1048576 | tf_op jit(solution)/shard_map/all_to_all | solution.py:72
  57.4 1.0 fusion.47
  59.7 11.3 %all-to-all-done = bf16[32,4,2048]{2,1,0:T(4,128)(2,1)} async-done(((bf16[32,4,2048]{2,1,0:T(4,128)(2,1)}), bf16[32,4,2048]{2,1,0:T(4,128)(2,1)}, u32[]{:S(2)}, u32[]{:S(2)}) %all-to-all-start) | async-done | bytes 524320 | tf_op jit(solution)/shard_map/all_to_all | solution.py:72
  71.0 2.1 %copy.14 = bf16[4,32,2048]{2,1,0:T(8,128)(2,1)} copy(bf16[4,32,2048]{2,0,1:T(4,128)(2,1)} %bitcast.5) | data formatting | bytes 1048576 | tf_op jit(solution)/shard_map/all_to_all | solution.py:72
  73.2 1.3 reshape.91
  74.5 1.5 fusion.38
  76.0 1.5 fusion.36
  77.5 1.6 convolution_add_fusion
  79.1 1.6 convolution_subtract_fusion
  80.7 2.1 %fusion.12 = f32[256,4,256]{2,0,1:T(8,128)S(1)} fusion(f32[256,4,256]{2,0,1:T(8,128)S(1)} %convolution_subtract_fusion, f32[256,4,256]{2,0,1:T(8,128)S(1)} %convolution_add_fusion, f32[256,256]{1,0:T(8,128)S(1)} %copy-done.3, f32[256,256]{1,0:T(8,128)S(1)} %copy.17), kind=kOutput, calls=%fused_computation.21 | convolution fusion | flops 807010304 | bytes 3670016 | tf_op jit(solution)/shard_map/ckq,qj->cjk/dot_general | solution.py:34
  82.8 2.4 %fusion.10 = bf16[4,256,256]{2,1,0:T(8,128)(2,1)S(1)} fusion(f32[256,4,256]{2,0,1:T(8,128)S(1)} %fusion.12, f32[256,4,256]{2,0,1:T(8,128)S(1)} %convolution_add_fusion, f32[256,4,256]{2,0,1:T(8,128)S(1)} %convolution_subtract_fusion, f32[256,256]{1,0:T(8,128)S(1)} %copy-done.3, f32[256,256]{1,0:T(8,128)S(1)} %copy.17), kind=kOutput, calls=%fused_computation.19 | convolution fusion | flops 807796736 | bytes 4194304 | tf_op jit(solution)/shard_map/ckq,qj->cjk/dot_general | solution.py:34
  85.9 21.5 %all_to_all.39 = bf16[4,32,2048]{2,0,1:T(4,128)(2,1)S(1)} all-to-all(bf16[4,32,2048]{2,0,1:T(4,128)(2,1)S(1)} %copy.19), channel_id=1, replica_groups=mesh['row'=32,'col'=8] {'row'}, dimensions={1} | all-to-all | bytes 1048576 | tf_op jit(solution)/shard_map/all_to_all | solution.py:79
  108.4 33.1 %all-gather.2.cloned.1.call-done = bf16[4096,512]{0,1:T(8,128)(2,1)} async-done(((bf16[4096,64]{0,1:T(8,128)(2,1)}), bf16[4096,512]{0,1:T(8,128)(2,1)}) %all-gather.2.cloned.1.call-update) | async-done | bytes 4194320 | tf_op jit(solution)/shard_map/all_gather | solution.py:18
  141.5 10.3 %fusion.102 = bf16[4096,1024]{1,0:T(8,128)(2,1)} fusion(bf16[4096,512]{0,1:T(8,128)(2,1)} %all-gather.2.cloned.1.call-done, bf16[512,1024]{1,0:T(8,128)(2,1)} %param.10), kind=kOutput, calls=%fused_computation.113 | convolution fusion | flops 4294967296 | bytes 13631488 | tf_op jit(solution)/shard_map/dot_general | solution.py:85
  151.8 16.7 %fusion.4 = bf16[4096,128]{1,0:T(8,128)(2,1)} fusion(bf16[1024,128]{1,0:T(8,128)(2,1)S(1)} %copy-done.6, bf16[4096,1024]{1,0:T(8,128)(2,1)} %bitcast.70, bf16[1024,1024]{1,0:T(8,128)(2,1)S(1)} %copy-done, bf16[4096,1024]{1,0:T(8,128)(2,1)} %fusion.102), kind=kOutput, calls=%fused_computation.7 | convolution fusion | flops 9689366528 | bytes 20185088 | tf_op jit(solution)/shard_map/dot_general | solution.py:92
  (26 shorter events, 5.7 us)
Async XLA Ops:
  6.5 145.3 %copy-start = (bf16[1024,1024]{1,0:T(8,128)(2,1)S(1)}, bf16[1024,1024]{1,0:T(8,128)(2,1)}, u32[]{:S(2)}) copy-start(bf16[1024,1024]{1,0:T(8,128)(2,1)} %param.9) | copy-start | bytes 6291460
  6.5 5.9 %copy-start.2 = (bf16[2,2048,1024]{2,1,0:T(8,128)(2,1)S(1)}, bf16[2,2048,1024]{2,1,0:T(8,128)(2,1)}, u32[]{:S(2)}) copy-start(bf16[2,2048,1024]{2,1,0:T(8,128)(2,1)} %param.6) | copy-start | bytes 25165828
  6.5 5.9 %copy-start.5 = (f32[1024]{0:T(1024)S(1)}, f32[1024]{0:T(1024)}, u32[]{:S(2)}) copy-start(f32[1024]{0:T(1024)} %param.7) | copy-start | bytes 12292
  12.5 5.4 %copy-start.4 = (bf16[1024,64]{0,1:T(8,128)(2,1)S(1)}, bf16[1024,64]{0,1:T(8,128)(2,1)}, u32[]{:S(2)}) copy-start(bf16[1024,64]{0,1:T(8,128)(2,1)} %param.8) | copy-start | bytes 393220
  14.7 3.2 %copy-start.1 = (bf16[2,2048,1024]{2,1,0:T(8,128)(2,1)}, bf16[2,2048,1024]{2,1,0:T(8,128)(2,1)S(1)}, u32[]{:S(2)}) copy-start(bf16[2,2048,1024]{2,1,0:T(8,128)(2,1)S(1)} %fusion.2) | copy-start | bytes 25165828
  22.2 28.1 %all-to-all-start.1 = ((bf16[32,4,2048]{2,1,0:T(4,128)(2,1)}), bf16[32,4,2048]{2,1,0:T(4,128)(2,1)S(1)}, u32[]{:S(2)}, u32[]{:S(2)}) async-start(bf16[32,4,2048]{2,1,0:T(4,128)(2,1)} %convert_element_type.107), calls=%async_computation.1 | async-start | bytes 1048576 | tf_op jit(solution)/shard_map/all_to_all | solution.py:75
  50.3 20.7 %all-to-all-start = ((bf16[32,4,2048]{2,1,0:T(4,128)(2,1)}), bf16[32,4,2048]{2,1,0:T(4,128)(2,1)}, u32[]{:S(2)}, u32[]{:S(2)}) async-start(bf16[32,4,2048]{2,1,0:T(4,128)(2,1)} %convert_element_type.103), calls=%async_computation | async-start | bytes 1048576 | tf_op jit(solution)/shard_map/all_to_all | solution.py:72
  56.0 85.5 %all-gather.2.cloned.1.call-start = ((), (), s32[]{:S(2)}) async-start(), calls=%async_computation.3 | async-start | bytes 4718592 | tf_op jit(solution)/shard_map/all_gather | solution.py:18
  74.5 6.2 %copy-start.3 = (f32[256,256]{1,0:T(8,128)S(1)}, f32[256,256]{1,0:T(8,128)}, u32[]{:S(2)}) copy-start(f32[256,256]{1,0:T(8,128)} %copy.18) | copy-start | bytes 786436
  108.4 43.4 %copy-start.6 = (bf16[1024,128]{1,0:T(8,128)(2,1)S(1)}, bf16[1024,128]{1,0:T(8,128)(2,1)}, u32[]{:S(2)}) copy-start(bf16[1024,128]{1,0:T(8,128)(2,1)} %param.11) | copy-start | bytes 786436
Sparse Core Ops, SparseCore 0:
  108.5 32.9 all-gather.1
where the time goes:
time: 176 us; the launch traced here: 175 us
  waiting for transfers between devices  56.9 us (32%)
  matrix products  42.6 us (24%)
  blocking collectives  21.5 us (12%)
  starting transfers between devices  17.9 us (10%)
  between operations  13.6 us (8%)
  local copies, waits for them, and re-layouts  13.4 us (8%)
  other arithmetic  9.39 us (5%)
    all_gather x1, waiting for transfers between devices, over_all(): lax.all_gather(part, axis, axis=dim, tiled=True)  33.1 us
    all_to_all x1, blocking collectives, on_device(): lax.all_to_all(spectrum, 'row', split_axis=1, concat_axis=0, tiled=True)  21.5 us
    dot_general x1, matrix products, on_device(): result = jnp.dot(mixed, w_output, preferred_element_type=jnp.float32)  16.7 us
    all_to_all x1, waiting for transfers between devices, on_device(): lax.all_to_all(shortened(imag_part), 'row', split_axis=0, concat_axis=1,...  12.5 us
    all_to_all x1, starting transfers between devices, on_device(): lax.all_to_all(shortened(imag_part), 'row', split_axis=0, concat_axis=1,...  12 us
    all_to_all x1, waiting for transfers between devices, on_device(): lax.all_to_all(shortened(real_part), 'row', split_axis=0, concat_axis=1,...  11.3 us
    dot_general x1, matrix products, add_spectrum(): jnp.dot(portion, weight_rows, preferred_element_type=jnp.float32)  10.3 us
    dot_general x4, matrix products, transform_first(): jnp.einsum('cpq,pk->ckq', cube, table, precision=lax.Precision.HIGHEST)  6.18 us
  transfers between devices with their start and end apart: 3, of which 3 were waited for; matrix products, arithmetic and copies ran while one was open for 4% of the time, Pallas kernels for 0%

commit v1 on v0

v1 whole, which is shorter than its diff:
```python
import functools

import jax
import jax.numpy as jnp
import numpy as np
from jax import lax
from jax.experimental import pallas as pl
from jax.experimental.pallas import tpu as pltpu
from jax.sharding import PartitionSpec as P

GROUP = 64
ROWS = 32
COLS = 8
SEQ = 65536
RADIX = 256
EPS = 1e-06
MESH = pl.DeviceIdType.MESH
BF16 = jnp.bfloat16
F32 = jnp.float32


def angles(left, right, period):
    return 2.0 * np.pi * (np.outer(left, right) % period) / period


def tables():
    n = np.arange(GROUP)
    channel = np.zeros((32, 2, GROUP))
    channel[:, 0] = np.cos(angles(np.arange(32), n, GROUP))
    channel[:, 1] = -np.sin(angles(np.arange(32), n, GROUP))
    channel[0, 1] = np.cos(angles(np.array([32]), n, GROUP))[0]
    spread = np.einsum("jan,pr->japrn", channel, np.eye(8)).reshape(512, 512)
    p = np.arange(RADIX)
    first_cos = np.cos(angles(p, p, RADIX))
    first_sin = -np.sin(angles(p, p, RADIX))
    first = np.zeros((2, 2, RADIX, 32, 2, 8))
    for part in range(2):
        first[part, 0, :, :, part] = first_cos.reshape(RADIX, 32, 8)
        first[part, 1, :, :, part] = first_sin.reshape(RADIX, 32, 8)
    first = first.reshape(1024, 512)
    twist = angles(p, p, SEQ)
    twist = np.stack([np.cos(twist), np.sin(twist)])
    second_cos = np.cos(angles(p, p, RADIX)) / 2048.0
    second_sin = np.sin(angles(p, p, RADIX)) / 2048.0
    second = np.stack(
        [
            np.concatenate([second_cos, second_sin], axis=1),
            np.concatenate([second_sin, -second_cos], axis=1),
        ]
    )
    bf = lambda a: jnp.asarray(a, dtype=F32).astype(BF16)
    return bf(spread), bf(first), jnp.asarray(twist, dtype=F32), bf(second)


def dot(a, b):
    return jnp.dot(a, b, preferred_element_type=F32)


def dot_nt(a, b):
    return lax.dot_general(a, b, (((1,), (1,)), ((), ())), preferred_element_type=F32)


def kernel(
    tok, gain, wfin, wgate, wspec, wout, spread, first, twist, second,
    out,
    x_v, gain_v, wfin_v, wgate_v, wspec_v, wout_v, spread_v, first_v, twist_v, second_v,
    wg_v, u_v, sig_v, perm_v, eye_v,
    send1, recv1, send2, recv2, send3, recv3, send4,
    x_sem, w_sem, ssem, rsem, wo_s, wo_r,
):
    row = lax.axis_index("row")
    col = lax.axis_index("col")
    chip = col // 2
    core = col % 2
    mate = chip * 2 + (1 - core)
    bar = pltpu.get_barrier_semaphore()

    def row_peer(d):
        return lax.rem(row + d, ROWS)

    def col_peer(d):
        return lax.rem(col + d, COLS)

    def signal_row(d, c):
        pl.semaphore_signal(bar, inc=1, device_id=(row_peer(d), col), device_id_type=MESH)
        return c

    def signal_col(d, c):
        pl.semaphore_signal(bar, inc=1, device_id=(row, col_peer(d)), device_id_type=MESH)
        return c

    lax.fori_loop(1, ROWS, signal_row, 0)
    lax.fori_loop(1, COLS, signal_col, 0)

    my_cols = pl.ds(pl.multiple_of(col * 128, 128), 128)
    loads = [
        pltpu.make_async_copy(gain, gain_v, w_sem.at[0]),
        pltpu.make_async_copy(wfin, wfin_v, w_sem.at[1]),
        pltpu.make_async_copy(spread, spread_v, w_sem.at[2]),
        pltpu.make_async_copy(wout, wout_v.at[:, my_cols], w_sem.at[3]),
        pltpu.make_async_copy(first, first_v, w_sem.at[4]),
        pltpu.make_async_copy(twist, twist_v, w_sem.at[5]),
        pltpu.make_async_copy(second, second_v, w_sem.at[6]),
        pltpu.make_async_copy(wgate, wgate_v, w_sem.at[7]),
        pltpu.make_async_copy(wspec, wspec_v, w_sem.at[8]),
    ]

    def tok_copy(b, i):
        return pltpu.make_async_copy(
            tok.at[b, pl.ds(pl.multiple_of(i * 512, 512), 512), :], x_v.at[b, i], x_sem.at[b, i]
        )

    loads[0].start()
    loads[1].start()
    for i in range(4):
        tok_copy(0, i).start()
    for i in (2, 3, 4, 5, 6):
        loads[i].start()
    for i in range(4):
        tok_copy(1, i).start()
    loads[7].start()
    loads[8].start()

    loads[0].wait()
    loads[1].wait()
    gain_col = jnp.transpose(jnp.broadcast_to(gain_v[...], (8, 1024)))[:, 0:1]
    wg_v[...] = (wfin_v[...].astype(F32) * gain_col).astype(BF16)

    def project(b):
        def body(i, c):
            tok_copy(b, i).wait()
            halves = []
            for h in range(2):
                x = x_v[b, i, pl.ds(h * 256, 256), :]
                wide = x.astype(F32)
                inv = lax.rsqrt(jnp.sum(wide * wide, axis=1, keepdims=True) * (1.0 / 1024) + EPS)
                halves.append(dot(x, wg_v[...]) * inv)
            u_v[b, :, pl.ds(pl.multiple_of(i * 128, 128), 128)] = jnp.concatenate(
                halves, axis=1
            ).astype(BF16)
            return c

        lax.fori_loop(0, 4, body, 0)
        send1[b] = dot_nt(spread_v[...], u_v[b]).astype(BF16)

    def rows16(i):
        return pl.ds(pl.multiple_of(i * 16, 16), 16)

    def row_exchange(src, dst, b, k):
        def send(d, c):
            t = row_peer(d)
            pltpu.make_async_remote_copy(
                src_ref=src.at[b, rows16(t), :],
                dst_ref=dst.at[b, rows16(row), :],
                send_sem=ssem.at[k, b],
                recv_sem=rsem.at[k, b],
                device_id=(t, col),
                device_id_type=MESH,
            ).start()
            return c

        lax.fori_loop(1, ROWS, send, 0)
        dst[b, rows16(row), :] = src[b, rows16(row), :]

    def row_wait(ref, sem, b):
        part = ref.at[b, pl.ds(0, 16 * (ROWS - 1)), :]
        pltpu.make_async_copy(part, part, sem).wait()

    loads[2].wait()
    project(0)
    pl.semaphore_wait(bar, ROWS - 1 + COLS - 1)
    row_exchange(send1, recv1, 0, 0)

    def wout_copy(source, target, sem):
        block = wout_v.at[:, pl.ds(pl.multiple_of(source * 128, 128), 128)]
        return pltpu.make_async_remote_copy(
            src_ref=block,
            dst_ref=block,
            send_sem=wo_s.at[sem],
            recv_sem=wo_r.at[sem],
            device_id=(row, target),
            device_id_type=MESH,
        )

    loads[3].wait()
    for d in (1, 3, 2):
        wout_copy(col, lax.rem(chip + d, 4) * 2 + core, 0).start()
    wout_copy(col, mate, 1).start()

    project(1)
    row_exchange(send1, recv1, 1, 0)

    perm_row = lax.broadcasted_iota(jnp.int32, (512, 512), 0)
    perm_col = lax.broadcasted_iota(jnp.int32, (512, 512), 1)
    pair = perm_col // 16
    chan = jnp.where(perm_col % 16 < 8, pair, jnp.where(pair == 0, 32, 64 - pair))
    perm_v[...] = jnp.where(perm_row == (perm_col % 8) * 64 + chan, 1.0, 0.0).astype(BF16)
    eye_v[...] = jnp.where(
        lax.broadcasted_iota(jnp.int32, (256, 256), 0)
        == lax.broadcasted_iota(jnp.int32, (256, 256), 1),
        1.0,
        0.0,
    ).astype(BF16)

    loads[7].wait()
    for b in range(2):
        wide = x_v[b, col // 2, pl.ds(pl.multiple_of((col % 2) * 256, 256), 256), :].astype(F32)
        inv = lax.rsqrt(jnp.sum(wide * wide, axis=1, keepdims=True) * (1.0 / 1024) + EPS)
        normed = (wide * inv * gain_v[...]).astype(BF16)
        sig_v[b] = jax.nn.sigmoid(dot(normed, wgate_v[...]))

    loads[4].wait()
    loads[5].wait()
    loads[6].wait()
    plain = row != 0
    mix01 = jnp.where(plain, 1.0, 0.0).astype(F32)
    mix11 = jnp.where(plain, -1.0, 1.0).astype(F32)
    odd = jnp.where(plain, 1, 0)

    def transform(b):
        section = dot(first_v[...], recv1[b])
        c = twist_v[0]
        s = twist_v[1]

        def turned(re, im):
            return jnp.concatenate([re * c + im * s, im * c - re * s], axis=1).astype(BF16)

        even_part = dot_nt(second_v[0], turned(section[0:256], section[256:512]))
        odd_part = dot_nt(second_v[odd], turned(section[512:768], section[768:1024]))
        one = even_part + mix01 * odd_part
        two = mix01 * even_part + mix11 * odd_part
        send2[b] = (
            jnp.concatenate([one.reshape(32, 8, 256), two.reshape(32, 8, 256)], axis=1)
            .reshape(512, 256)
            .astype(BF16)
        )

    for b in range(2):
        row_wait(recv1, rsem.at[0, b], b)
        transform(b)
        row_exchange(send2, recv2, b, 1)

    got = wout_v.at[:, pl.ds(0, 384)]
    pltpu.make_async_copy(got, got, wo_r.at[0]).wait()
    for d in (1, 2, 3):
        wout_copy(lax.rem(chip + d, 4) * 2 + core, mate, 1).start()

    def rows64(i):
        return pl.ds(pl.multiple_of(i * 64, 64), 64)

    def spread_tokens(b):
        row_wait(recv2, rsem.at[1, b], b)
        send3[b] = dot(perm_v[...], recv2[b]).astype(BF16)

        def send(d, c):
            t = col_peer(d)
            pltpu.make_async_remote_copy(
                src_ref=send3.at[b, rows64(t), :],
                dst_ref=recv3.at[b, rows64(col), :],
                send_sem=ssem.at[2, b],
                recv_sem=rsem.at[2, b],
                device_id=(row, t),
                device_id_type=MESH,
            ).start()
            return c

        lax.fori_loop(1, COLS, send, 0)
        recv3[b, rows64(col), :] = send3[b, rows64(col), :]

    def finish(b):
        part = recv3.at[b, pl.ds(0, 448), :]
        pltpu.make_async_copy(part, part, rsem.at[2, b]).wait()
        spectrum = dot_nt(eye_v[...], recv3[b]).astype(BF16)
        mixed_pre = dot(spectrum, wspec_v[...]).astype(BF16).astype(F32)
        mixed = (sig_v[b] * mixed_pre).astype(BF16)
        result = dot(mixed, wout_v[...]).astype(BF16)
        for t in range(COLS):
            send4[b, t] = result[:, t * 128 : (t + 1) * 128]

        def send(d, c):
            t = col_peer(d)
            pltpu.make_async_remote_copy(
                src_ref=send4.at[b, t],
                dst_ref=out.at[b, pl.ds(pl.multiple_of(col * 256, 256), 256), :],
                send_sem=ssem.at[3, b],
                recv_sem=rsem.at[3, b],
                device_id=(row, t),
                device_id_type=MESH,
            ).start()
            return c

        lax.fori_loop(1, COLS, send, 0)
        out[b, pl.ds(pl.multiple_of(col * 256, 256), 256), :] = send4[b, col]

    spread_tokens(0)
    loads[8].wait()
    mates = wout_v.at[:, pl.ds(0, 512)]
    pltpu.make_async_copy(mates, mates, wo_r.at[1]).wait()
    finish(0)
    spread_tokens(1)
    finish(1)

    for b in range(2):
        part = out.at[b, pl.ds(0, 1792), :]
        pltpu.make_async_copy(part, part, rsem.at[3, b]).wait()
        row_wait(send1, ssem.at[0, b], b)
        row_wait(send2, ssem.at[1, b], b)
        part = send3.at[b, pl.ds(0, 448), :]
        pltpu.make_async_copy(part, part, ssem.at[2, b]).wait()
        part = send4.at[b, pl.ds(0, 7)]
        pltpu.make_async_copy(part, part, ssem.at[3, b]).wait()
    pltpu.make_async_copy(got, got, wo_s.at[0]).wait()
    pltpu.make_async_copy(mates, mates, wo_s.at[1]).wait()


def on_device(tokens, norm_gain, w_fourier_in, w_gate, w_spectrum, w_output):
    spread, first, twist, second = tables()
    vmem = pltpu.VMEM
    return pl.pallas_call(
        kernel,
        out_shape=jax.ShapeDtypeStruct((2, 2048, 128), BF16),
        in_specs=[pl.BlockSpec(memory_space=pl.ANY)] * 10,
        out_specs=pl.BlockSpec(memory_space=pltpu.VMEM),
        scratch_shapes=[
            vmem((2, 4, 512, 1024), BF16),
            vmem((1, 1024), F32),
            vmem((1024, 64), BF16),
            vmem((1024, 1024), BF16),
            vmem((512, 1024), BF16),
            vmem((1024, 1024), BF16),
            vmem((512, 512), BF16),
            vmem((1024, 512), BF16),
            vmem((2, 256, 256), F32),
            vmem((2, 256, 512), BF16),
            vmem((1024, 64), BF16),
            vmem((2, 256, 512), BF16),
            vmem((2, 256, 1024), F32),
            vmem((512, 512), BF16),
            vmem((256, 256), BF16),
            vmem((2, 512, 256), BF16),
            vmem((2, 512, 256), BF16),
            vmem((2, 512, 256), BF16),
            vmem((2, 512, 256), BF16),
            vmem((2, 512, 256), BF16),
            vmem((2, 512, 256), BF16),
            vmem((2, 8, 256, 128), BF16),
            pltpu.SemaphoreType.DMA((2, 4)),
            pltpu.SemaphoreType.DMA((9,)),
            pltpu.SemaphoreType.DMA((4, 2)),
            pltpu.SemaphoreType.DMA((4, 2)),
            pltpu.SemaphoreType.DMA((2,)),
            pltpu.SemaphoreType.DMA((2,)),
        ],
        compiler_params=pltpu.CompilerParams(
            collective_id=0, has_side_effects=True, vmem_limit_bytes=60 << 20
        ),
    )(
        tokens, norm_gain.reshape(1, 1024), w_fourier_in, w_gate, w_spectrum, w_output,
        spread, first, twist, second,
    )


def solution(mesh):
    placed = (P(None, "row", None), P(), P(None, "col"), P(), P(), P(None, "col"))
    return jax.shard_map(
        on_device, mesh=mesh, in_specs=placed, out_specs=P(None, "row", "col"), check_vma=False
    )
```

time: 176 us -> 65.7 us (0.37)
  Pallas kernels: 0 us -> 61.5 us
  waiting for transfers between devices: 56.9 us -> 0 us
  matrix products: 42.6 us -> 0 us
  blocking collectives: 21.5 us -> 0 us
  starting transfers between devices: 17.9 us -> 0 us
  between operations: 13.6 us -> 0.01 us
  other arithmetic: 9.39 us -> 0 us
  local copies, waits for them, and re-layouts: 13.4 us -> 4.01 us
    pallas_call x0 -> x1, Pallas kernels: none -> 61.5 us  [on_device(): pl.pallas_call(kernel, out_shape=jax.ShapeDtypeStruct((2, 2048, 128), BF1...]
    dot_general x11 -> x0, matrix products: 42.6 us -> none  [the longest x1 16.7 us: on_device(): result = jnp.dot(mixed, w_output, preferred_element_type=jnp.float32)]
    all_gather x1 -> x0, waiting for transfers between devices: 33.1 us -> none  [over_all(): lax.all_gather(part, axis, axis=dim, tiled=True)]
    all_to_all x2 -> x0, waiting for transfers between devices: 23.8 us -> none  [the longest x1 12.5 us: on_device(): lax.all_to_all(shortened(imag_part), 'row', split_axis=0, concat_axis=1,...]
    all_to_all x1 -> x0, blocking collectives: 21.5 us -> none  [on_device(): lax.all_to_all(spectrum, 'row', split_axis=1, concat_axis=0, tiled=True)]
    all_to_all x2 -> x0, starting transfers between devices: 17.7 us -> none  [the longest x1 12 us: on_device(): lax.all_to_all(shortened(imag_part), 'row', split_axis=0, concat_axis=1,...]
    reduce_sum x1 -> x0, other arithmetic: 5.25 us -> none  [on_device(): jnp.mean(widened * widened, axis=-1, keepdims=True) + norm_eps]
    convert_element_type x4 -> x0, local copies, waits for them, and re-layouts: 3.69 us -> none  [the longest x2 3.04 us: shortened(): a.astype(jnp.bfloat16)]
  transfers between devices with their start and end apart: 3 -> 0, of which waited for: 3 -> 0; matrix products, arithmetic and copies ran while one was open for 4% -> 0% of each run, Pallas kernels for 0% -> 0%
where the time goes in v1:
time: 65.7 us; the launch traced here: 65.5 us
  Pallas kernels  61.5 us (94%)
  local copies, waits for them, and re-layouts  4.01 us (6%)
    pallas_call x1, Pallas kernels, on_device(): pl.pallas_call(kernel, out_shape=jax.ShapeDtypeStruct((2, 2048, 128), BF1...  61.5 us
    unnamed x2, local copies, waits for them, and re-layouts  4.01 us

profile of v1, /device:TPU:1, one launch (start us, length us, event | category | flops | bytes accessed | tf_op | source)
XLA Modules:
  0.0 65.5 jit_solution(10416793756999874263)
XLA Ops:
  0.0 1.7 %copy.11.wfin = bf16[1024,64]{1,0:T(8,128)(2,1)} copy(bf16[1024,64]{0,1:T(8,128)(2,1)} %param.12) | data formatting | bytes 262144 | tf_op args[2]
  1.7 61.5 %shard_map.100 = bf16[2,2048,128]{2,1,0:T(8,128)(2,1)} custom-call(bf16[2,2048,1024]{2,1,0:T(8,128)(2,1)} %tok.1, f32[1,1024]{1,0:T(1,128)} %bitcast.1, bf16[1024,64]{1,0:T(8,128)(2,1)} %copy.11.wfin, bf16[1024,1024]{1,0:T(8,128)(2,1)} %wgate.1, bf16[512,1024]{1,0:T(8,128)(2,1)} %wspec.1, bf16[1024,128]{1,0:T(8,128)(2,1)} %wout.1, ...), custom_call_target="tpu_custom_call" | custom-call | tf_op jit(solution)/shard_map/pallas_call | solution.py:319
  63.3 2.3 %copy.13 = bf16[2,2048,128]{2,1,0:T(8,128)(2,1)} copy(bf16[2,2048,128]{2,1,0:T(8,128)(2,1)} %shard_map.100) | data formatting | bytes 2097152

commit v2 on v1

--- a/solution.py
+++ b/solution.py
@@ -66,7 +66,7 @@
     x_v, gain_v, wfin_v, wgate_v, wspec_v, wout_v, spread_v, first_v, twist_v, second_v,
     wg_v, u_v, sig_v, perm_v, eye_v,
     send1, recv1, send2, recv2, send3, recv3, send4,
-    x_sem, w_sem, ssem, rsem, wo_s, wo_r,
+    x_sem, w_sem, s1, r1, s2, r2, s3, r3, s4, r4, wo_s, wo_r,
 ):
     row = lax.axis_index("row")
     col = lax.axis_index("col")
@@ -123,8 +123,7 @@
 
     loads[0].wait()
     loads[1].wait()
-    gain_col = jnp.transpose(jnp.broadcast_to(gain_v[...], (8, 1024)))[:, 0:1]
-    wg_v[...] = (wfin_v[...].astype(F32) * gain_col).astype(BF16)
+    wg_v[...] = (wfin_v[...].astype(F32) * gain_v[...]).astype(BF16)
 
     def project(b):
         def body(i, c):
@@ -134,7 +133,7 @@
                 x = x_v[b, i, pl.ds(h * 256, 256), :]
                 wide = x.astype(F32)
                 inv = lax.rsqrt(jnp.sum(wide * wide, axis=1, keepdims=True) * (1.0 / 1024) + EPS)
-                halves.append(dot(x, wg_v[...]) * inv)
+                halves.append(dot_nt(x, wg_v[...]) * inv)
             u_v[b, :, pl.ds(pl.multiple_of(i * 128, 128), 128)] = jnp.concatenate(
                 halves, axis=1
             ).astype(BF16)
@@ -146,30 +145,32 @@
     def rows16(i):
         return pl.ds(pl.multiple_of(i * 16, 16), 16)
 
-    def row_exchange(src, dst, b, k):
+    def row_exchange(src, dst, send_sem, recv_sem):
         def send(d, c):
             t = row_peer(d)
             pltpu.make_async_remote_copy(
-                src_ref=src.at[b, rows16(t), :],
-                dst_ref=dst.at[b, rows16(row), :],
-                send_sem=ssem.at[k, b],
-                recv_sem=rsem.at[k, b],
+                src_ref=src.at[rows16(t), :],
+                dst_ref=dst.at[rows16(row), :],
+                send_sem=send_sem,
+                recv_sem=recv_sem,
                 device_id=(t, col),
                 device_id_type=MESH,
             ).start()
             return c
 
         lax.fori_loop(1, ROWS, send, 0)
-        dst[b, rows16(row), :] = src[b, rows16(row), :]
-
-    def row_wait(ref, sem, b):
-        part = ref.at[b, pl.ds(0, 16 * (ROWS - 1)), :]
+        dst[rows16(row), :] = src[rows16(row), :]
+
+    def wait_for(part, sem):
         pltpu.make_async_copy(part, part, sem).wait()
+
+    def row_wait(ref, sem):
+        wait_for(ref.at[pl.ds(0, 16 * (ROWS - 1)), :], sem)
 
     loads[2].wait()
     project(0)
     pl.semaphore_wait(bar, ROWS - 1 + COLS - 1)
-    row_exchange(send1, recv1, 0, 0)
+    row_exchange(send1.at[0], recv1.at[0], s1.at[0], r1.at[0])
 
     def wout_copy(source, target, sem):
         block = wout_v.at[:, pl.ds(pl.multiple_of(source * 128, 128), 128)]
@@ -188,7 +189,7 @@
     wout_copy(col, mate, 1).start()
 
     project(1)
-    row_exchange(send1, recv1, 1, 0)
+    row_exchange(send1.at[1], recv1.at[1], s1.at[1], r1.at[1])
 
     perm_row = lax.broadcasted_iota(jnp.int32, (512, 512), 0)
     perm_col = lax.broadcasted_iota(jnp.int32, (512, 512), 1)
@@ -196,8 +197,8 @@
     chan = jnp.where(perm_col % 16 < 8, pair, jnp.where(pair == 0, 32, 64 - pair))
     perm_v[...] = jnp.where(perm_row == (perm_col % 8) * 64 + chan, 1.0, 0.0).astype(BF16)
     eye_v[...] = jnp.where(
-        lax.broadcasted_iota(jnp.int32, (256, 256), 0)
-        == lax.broadcasted_iota(jnp.int32, (256, 256), 1),
+        lax.broadcasted_iota(jnp.int32, (128, 128), 0)
+        == lax.broadcasted_iota(jnp.int32, (128, 128), 1),
         1.0,
         0.0,
     ).astype(BF16)
@@ -229,88 +230,91 @@
         odd_part = dot_nt(second_v[odd], turned(section[512:768], section[768:1024]))
         one = even_part + mix01 * odd_part
         two = mix01 * even_part + mix11 * odd_part
-        send2[b] = (
+        both = (
             jnp.concatenate([one.reshape(32, 8, 256), two.reshape(32, 8, 256)], axis=1)
             .reshape(512, 256)
             .astype(BF16)
         )
+        for h in range(2):
+            send2[b, h] = both[:, h * 128 : (h + 1) * 128]
 
     for b in range(2):
-        row_wait(recv1, rsem.at[0, b], b)
+        row_wait(recv1.at[b], r1.at[b])
         transform(b)
-        row_exchange(send2, recv2, b, 1)
-
-    got = wout_v.at[:, pl.ds(0, 384)]
-    pltpu.make_async_copy(got, got, wo_r.at[0]).wait()
+        for h in range(2):
+            row_exchange(send2.at[b, h], recv2.at[b, h], s2.at[b, h], r2.at[b, h])
+
+    wait_for(wout_v.at[:, pl.ds(0, 384)], wo_r.at[0])
     for d in (1, 2, 3):
         wout_copy(lax.rem(chip + d, 4) * 2 + core, mate, 1).start()
 
     def rows64(i):
         return pl.ds(pl.multiple_of(i * 64, 64), 64)
 
-    def spread_tokens(b):
-        row_wait(recv2, rsem.at[1, b], b)
-        send3[b] = dot(perm_v[...], recv2[b]).astype(BF16)
+    def spread_tokens(b, h):
+        row_wait(recv2.at[b, h], r2.at[b, h])
+        send3[b, h] = dot(perm_v[...], recv2[b, h]).astype(BF16)
 
         def send(d, c):
             t = col_peer(d)
             pltpu.make_async_remote_copy(
-                src_ref=send3.at[b, rows64(t), :],
-                dst_ref=recv3.at[b, rows64(col), :],
-                send_sem=ssem.at[2, b],
-                recv_sem=rsem.at[2, b],
+                src_ref=send3.at[b, h, rows64(t), :],
+                dst_ref=recv3.at[b, h, rows64(col), :],
+                send_sem=s3.at[b, h],
+                recv_sem=r3.at[b, h],
                 device_id=(row, t),
                 device_id_type=MESH,
             ).start()
             return c
 
         lax.fori_loop(1, COLS, send, 0)
-        recv3[b, rows64(col), :] = send3[b, rows64(col), :]
-
-    def finish(b):
-        part = recv3.at[b, pl.ds(0, 448), :]
-        pltpu.make_async_copy(part, part, rsem.at[2, b]).wait()
-        spectrum = dot_nt(eye_v[...], recv3[b]).astype(BF16)
+        recv3[b, h, rows64(col), :] = send3[b, h, rows64(col), :]
+
+    def finish(b, h):
+        wait_for(recv3.at[b, h, pl.ds(0, 448), :], r3.at[b, h])
+        spectrum = dot_nt(eye_v[...], recv3[b, h]).astype(BF16)
         mixed_pre = dot(spectrum, wspec_v[...]).astype(BF16).astype(F32)
-        mixed = (sig_v[b] * mixed_pre).astype(BF16)
+        mixed = (sig_v[b, h * 128 : (h + 1) * 128] * mixed_pre).astype(BF16)
         result = dot(mixed, wout_v[...]).astype(BF16)
         for t in range(COLS):
-            send4[b, t] = result[:, t * 128 : (t + 1) * 128]
+            send4[b, h, t] = result[:, t * 128 : (t + 1) * 128]
+        place = pl.ds(pl.multiple_of(col * 256 + h * 128, 128), 128)
 
         def send(d, c):
             t = col_peer(d)
             pltpu.make_async_remote_copy(
-                src_ref=send4.at[b, t],
-                dst_ref=out.at[b, pl.ds(pl.multiple_of(col * 256, 256), 256), :],
-                send_sem=ssem.at[3, b],
-                recv_sem=rsem.at[3, b],
+                src_ref=send4.at[b, h, t],
+                dst_ref=out.at[b, place, :],
+                send_sem=s4.at[b, h],
+                recv_sem=r4.at[b, h],
                 device_id=(row, t),
                 device_id_type=MESH,
             ).start()
             return c
 
         lax.fori_loop(1, COLS, send, 0)
-        out[b, pl.ds(pl.multiple_of(col * 256, 256), 256), :] = send4[b, col]
-
-    spread_tokens(0)
+        out[b, place, :] = send4[b, h, col]
+
+    spread_tokens(0, 0)
     loads[8].wait()
-    mates = wout_v.at[:, pl.ds(0, 512)]
-    pltpu.make_async_copy(mates, mates, wo_r.at[1]).wait()
-    finish(0)
-    spread_tokens(1)
-    finish(1)
+    wait_for(wout_v.at[:, pl.ds(0, 512)], wo_r.at[1])
+    spread_tokens(0, 1)
+    finish(0, 0)
+    spread_tokens(1, 0)
+    finish(0, 1)
+    spread_tokens(1, 1)
+    finish(1, 0)
+    finish(1, 1)
 
     for b in range(2):
-        part = out.at[b, pl.ds(0, 1792), :]
-        pltpu.make_async_copy(part, part, rsem.at[3, b]).wait()
-        row_wait(send1, ssem.at[0, b], b)
-        row_wait(send2, ssem.at[1, b], b)
-        part = send3.at[b, pl.ds(0, 448), :]
-        pltpu.make_async_copy(part, part, ssem.at[2, b]).wait()
-        part = send4.at[b, pl.ds(0, 7)]
-        pltpu.make_async_copy(part, part, ssem.at[3, b]).wait()
-    pltpu.make_async_copy(got, got, wo_s.at[0]).wait()
-    pltpu.make_async_copy(mates, mates, wo_s.at[1]).wait()
+        row_wait(send1.at[b], s1.at[b])
+        for h in range(2):
+            row_wait(send2.at[b, h], s2.at[b, h])
+            wait_for(send3.at[b, h, pl.ds(0, 448), :], s3.at[b, h])
+            wait_for(send4.at[b, h, pl.ds(0, 7)], s4.at[b, h])
+            wait_for(out.at[b, pl.ds(0, 896), :], r4.at[b, h])
+    wait_for(wout_v.at[:, pl.ds(0, 384)], wo_s.at[0])
+    wait_for(wout_v.at[:, pl.ds(0, 512)], wo_s.at[1])
 
 
 def on_device(tokens, norm_gain, w_fourier_in, w_gate, w_spectrum, w_output):
@@ -318,13 +322,13 @@
     vmem = pltpu.VMEM
     return pl.pallas_call(
         kernel,
-        out_shape=jax.ShapeDtypeStruct((2, 2048, 128), BF16),
+        out_shape=vmem((2, 2048, 128), BF16),
         in_specs=[pl.BlockSpec(memory_space=pl.ANY)] * 10,
         out_specs=pl.BlockSpec(memory_space=pltpu.VMEM),
         scratch_shapes=[
             vmem((2, 4, 512, 1024), BF16),
             vmem((1, 1024), F32),
-            vmem((1024, 64), BF16),
+            vmem((64, 1024), BF16),
             vmem((1024, 1024), BF16),
             vmem((512, 1024), BF16),
             vmem((1024, 1024), BF16),
@@ -332,22 +336,20 @@
             vmem((1024, 512), BF16),
             vmem((2, 256, 256), F32),
             vmem((2, 256, 512), BF16),
-            vmem((1024, 64), BF16),
+            vmem((64, 1024), BF16),
             vmem((2, 256, 512), BF16),
             vmem((2, 256, 1024), F32),
             vmem((512, 512), BF16),
-            vmem((256, 256), BF16),
+            vmem((128, 128), BF16),
             vmem((2, 512, 256), BF16),
             vmem((2, 512, 256), BF16),
-            vmem((2, 512, 256), BF16),
-            vmem((2, 512, 256), BF16),
-            vmem((2, 512, 256), BF16),
-            vmem((2, 512, 256), BF16),
-            vmem((2, 8, 256, 128), BF16),
+            *[vmem((2, 2, 512, 128), BF16)] * 4,
+            vmem((2, 2, 8, 128, 128), BF16),
             pltpu.SemaphoreType.DMA((2, 4)),
             pltpu.SemaphoreType.DMA((9,)),
-            pltpu.SemaphoreType.DMA((4, 2)),
-            pltpu.SemaphoreType.DMA((4, 2)),
+            pltpu.SemaphoreType.DMA((2,)),
+            pltpu.SemaphoreType.DMA((2,)),
+            *[pltpu.SemaphoreType.DMA((2, 2))] * 6,
             pltpu.SemaphoreType.DMA((2,)),
             pltpu.SemaphoreType.DMA((2,)),
         ],
@@ -355,7 +357,7 @@
             collective_id=0, has_side_effects=True, vmem_limit_bytes=60 << 20
         ),
     )(
-        tokens, norm_gain.reshape(1, 1024), w_fourier_in, w_gate, w_spectrum, w_output,
+        tokens, norm_gain.reshape(1, 1024), w_fourier_in.T, w_gate, w_spectrum, w_output,
         spread, first, twist, second,
     )
 

time: 65.7 us -> 56.2 us (0.86)
  Pallas kernels: 61.5 us -> 55.1 us
  local copies, waits for them, and re-layouts: 4.01 us -> 0.97 us
    pallas_call x1, Pallas kernels: 61.5 us -> 55.1 us  [on_device(): pl.pallas_call(kernel, out_shape=vmem((2, 2048, 128), BF16), in_specs=[pl...]
    unnamed x2 -> x1, local copies, waits for them, and re-layouts: 4.01 us -> 0.97 us
where the time goes in v2:
time: 56.2 us; the launch traced here: 56.1 us
  Pallas kernels  55.1 us (98%)
  local copies, waits for them, and re-layouts  0.97 us (2%)
    pallas_call x1, Pallas kernels, on_device(): pl.pallas_call(kernel, out_shape=vmem((2, 2048, 128), BF16), in_specs=[pl...  55.1 us

profile of v2, /device:TPU:1, one launch (start us, length us, event | category | flops | bytes accessed | tf_op | source)
XLA Modules:
  0.0 56.1 jit_solution(15038973232010218226)
XLA Ops:
  0.0 55.1 %shard_map.100 = bf16[2,2048,128]{2,1,0:T(8,128)(2,1)S(1)} custom-call(bf16[2,2048,1024]{2,1,0:T(8,128)(2,1)} %tok.1, f32[1,1024]{1,0:T(1,128)} %bitcast.3, bf16[64,1024]{1,0:T(8,128)(2,1)} %bitcast.2, bf16[1024,1024]{1,0:T(8,128)(2,1)} %wgate.1, bf16[512,1024]{1,0:T(8,128)(2,1)} %wspec.1, bf16[1024,128]{1,0:T(8,128)(2,1)} %wout.1, ...), custom_call_target="tpu_custom_call" | custom-call | tf_op jit(solution)/shard_map/pallas_call | solution.py:323
  55.1 1.0 %copy.12 = bf16[2,2048,128]{2,1,0:T(8,128)(2,1)} copy(bf16[2,2048,128]{2,1,0:T(8,128)(2,1)S(1)} %shard_map.100) | data formatting | bytes 2097152

commit v3 on v2

--- a/solution.py
+++ b/solution.py
@@ -48,6 +48,7 @@
             np.concatenate([second_sin, -second_cos], axis=1),
         ]
     )
+    second = second.reshape(2, 32, 8, 512).transpose(0, 2, 1, 3).reshape(2, 256, 512)
     bf = lambda a: jnp.asarray(a, dtype=F32).astype(BF16)
     return bf(spread), bf(first), jnp.asarray(twist, dtype=F32), bf(second)
 
@@ -63,7 +64,7 @@
 def kernel(
     tok, gain, wfin, wgate, wspec, wout, spread, first, twist, second,
     out,
-    x_v, gain_v, wfin_v, wgate_v, wspec_v, wout_v, spread_v, first_v, twist_v, second_v,
+    x_v, gain_v, wfin_v, wgate_v, wspec_v, wspec_p, wout_v, spread_v, first_v, twist_v, second_v,
     wg_v, u_v, sig_v, perm_v, eye_v,
     send1, recv1, send2, recv2, send3, recv3, send4,
     x_sem, w_sem, s1, r1, s2, r2, s3, r3, s4, r4, wo_s, wo_r,
@@ -172,8 +173,8 @@
     pl.semaphore_wait(bar, ROWS - 1 + COLS - 1)
     row_exchange(send1.at[0], recv1.at[0], s1.at[0], r1.at[0])
 
-    def wout_copy(source, target, sem):
-        block = wout_v.at[:, pl.ds(pl.multiple_of(source * 128, 128), 128)]
+    def wout_copy(part, source, target, sem):
+        block = wout_v.at[part, pl.ds(pl.multiple_of(source * 128, 128), 128)]
         return pltpu.make_async_remote_copy(
             src_ref=block,
             dst_ref=block,
@@ -183,19 +184,39 @@
             device_id_type=MESH,
         )
 
+    parts = (pl.ds(0, 672), pl.ds(672, 352))
+
+    def wout_out(k):
+        for d in (1, 3, 2):
+            wout_copy(parts[k], col, lax.rem(chip + d, 4) * 2 + core, k).start()
+
+    def wout_on(k):
+        wait_for(wout_v.at[parts[k], pl.ds(0, 384)], wo_r.at[k])
+        for d in (1, 2, 3):
+            wout_copy(parts[k], lax.rem(chip + d, 4) * 2 + core, mate, 2).start()
+
     loads[3].wait()
-    for d in (1, 3, 2):
-        wout_copy(col, lax.rem(chip + d, 4) * 2 + core, 0).start()
-    wout_copy(col, mate, 1).start()
+    wout_out(0)
+    wout_copy(pl.ds(0, 1024), col, mate, 2).start()
 
     project(1)
     row_exchange(send1.at[1], recv1.at[1], s1.at[1], r1.at[1])
 
-    perm_row = lax.broadcasted_iota(jnp.int32, (512, 512), 0)
-    perm_col = lax.broadcasted_iota(jnp.int32, (512, 512), 1)
-    pair = perm_col // 16
-    chan = jnp.where(perm_col % 16 < 8, pair, jnp.where(pair == 0, 32, 64 - pair))
-    perm_v[...] = jnp.where(perm_row == (perm_col % 8) * 64 + chan, 1.0, 0.0).astype(BF16)
+    iota_row = lax.broadcasted_iota(jnp.int32, (512, 512), 0)
+    iota_col = lax.broadcasted_iota(jnp.int32, (512, 512), 1)
+
+    def chosen(hit):
+        return jnp.where(hit, 1.0, 0.0).astype(BF16)
+
+    perm_v[...] = chosen(
+        iota_row == (iota_col % 32) * 16 + (iota_col // 64) * 2 + (iota_col % 64) // 32
+    )
+    pair = iota_row // 16
+    chan = jnp.where(iota_row % 2 == 0, pair, jnp.where(pair == 0, 32, 64 - pair))
+    loads[8].wait()
+    wspec_p[...] = dot(
+        chosen(iota_col == (iota_row % 16) // 2 * 64 + chan), wspec_v[...]
+    ).astype(BF16)
     eye_v[...] = jnp.where(
         lax.broadcasted_iota(jnp.int32, (128, 128), 0)
         == lax.broadcasted_iota(jnp.int32, (128, 128), 1),
@@ -231,49 +252,42 @@
         one = even_part + mix01 * odd_part
         two = mix01 * even_part + mix11 * odd_part
         both = (
-            jnp.concatenate([one.reshape(32, 8, 256), two.reshape(32, 8, 256)], axis=1)
+            jnp.concatenate([one.reshape(8, 32, 256), two.reshape(8, 32, 256)], axis=1)
             .reshape(512, 256)
             .astype(BF16)
         )
         for h in range(2):
             send2[b, h] = both[:, h * 128 : (h + 1) * 128]
-
-    for b in range(2):
-        row_wait(recv1.at[b], r1.at[b])
-        transform(b)
-        for h in range(2):
-            row_exchange(send2.at[b, h], recv2.at[b, h], s2.at[b, h], r2.at[b, h])
-
-    wait_for(wout_v.at[:, pl.ds(0, 384)], wo_r.at[0])
-    for d in (1, 2, 3):
-        wout_copy(lax.rem(chip + d, 4) * 2 + core, mate, 1).start()
+            col_exchange(send2.at[b, h], recv2.at[b, h], s2.at[b, h], r2.at[b, h])
 
     def rows64(i):
         return pl.ds(pl.multiple_of(i * 64, 64), 64)
 
-    def spread_tokens(b, h):
-        row_wait(recv2.at[b, h], r2.at[b, h])
-        send3[b, h] = dot(perm_v[...], recv2[b, h]).astype(BF16)
-
+    def col_exchange(src, dst, send_sem, recv_sem):
         def send(d, c):
             t = col_peer(d)
             pltpu.make_async_remote_copy(
-                src_ref=send3.at[b, h, rows64(t), :],
-                dst_ref=recv3.at[b, h, rows64(col), :],
-                send_sem=s3.at[b, h],
-                recv_sem=r3.at[b, h],
+                src_ref=src.at[rows64(t), :],
+                dst_ref=dst.at[rows64(col), :],
+                send_sem=send_sem,
+                recv_sem=recv_sem,
                 device_id=(row, t),
                 device_id_type=MESH,
             ).start()
             return c
 
         lax.fori_loop(1, COLS, send, 0)
-        recv3[b, h, rows64(col), :] = send3[b, h, rows64(col), :]
+        dst[rows64(col), :] = src[rows64(col), :]
+
+    def give_back(b, h):
+        wait_for(recv2.at[b, h, pl.ds(0, 448), :], r2.at[b, h])
+        send3[b, h] = dot(perm_v[...], recv2[b, h]).astype(BF16)
+        row_exchange(send3.at[b, h], recv3.at[b, h], s3.at[b, h], r3.at[b, h])
 
     def finish(b, h):
-        wait_for(recv3.at[b, h, pl.ds(0, 448), :], r3.at[b, h])
+        row_wait(recv3.at[b, h], r3.at[b, h])
         spectrum = dot_nt(eye_v[...], recv3[b, h]).astype(BF16)
-        mixed_pre = dot(spectrum, wspec_v[...]).astype(BF16).astype(F32)
+        mixed_pre = dot(spectrum, wspec_p[...]).astype(BF16).astype(F32)
         mixed = (sig_v[b, h * 128 : (h + 1) * 128] * mixed_pre).astype(BF16)
         result = dot(mixed, wout_v[...]).astype(BF16)
         for t in range(COLS):
@@ -295,26 +309,33 @@
         lax.fori_loop(1, COLS, send, 0)
         out[b, place, :] = send4[b, h, col]
 
-    spread_tokens(0, 0)
-    loads[8].wait()
-    wait_for(wout_v.at[:, pl.ds(0, 512)], wo_r.at[1])
-    spread_tokens(0, 1)
+    row_wait(recv1.at[0], r1.at[0])
+    transform(0)
+    wout_out(1)
+    give_back(0, 0)
+    row_wait(recv1.at[1], r1.at[1])
+    transform(1)
+    give_back(0, 1)
+    wout_on(0)
+    wout_on(1)
+    give_back(1, 0)
+    give_back(1, 1)
+    wait_for(wout_v.at[:, pl.ds(0, 512)], wo_r.at[2])
     finish(0, 0)
-    spread_tokens(1, 0)
     finish(0, 1)
-    spread_tokens(1, 1)
     finish(1, 0)
     finish(1, 1)
 
     for b in range(2):
         row_wait(send1.at[b], s1.at[b])
         for h in range(2):
-            row_wait(send2.at[b, h], s2.at[b, h])
-            wait_for(send3.at[b, h, pl.ds(0, 448), :], s3.at[b, h])
+            wait_for(send2.at[b, h, pl.ds(0, 448), :], s2.at[b, h])
+            row_wait(send3.at[b, h], s3.at[b, h])
             wait_for(send4.at[b, h, pl.ds(0, 7)], s4.at[b, h])
             wait_for(out.at[b, pl.ds(0, 896), :], r4.at[b, h])
-    wait_for(wout_v.at[:, pl.ds(0, 384)], wo_s.at[0])
-    wait_for(wout_v.at[:, pl.ds(0, 512)], wo_s.at[1])
+    for k in range(2):
+        wait_for(wout_v.at[parts[k], pl.ds(0, 384)], wo_s.at[k])
+    wait_for(wout_v.at[:, pl.ds(0, 512)], wo_s.at[2])
 
 
 def on_device(tokens, norm_gain, w_fourier_in, w_gate, w_spectrum, w_output):
@@ -330,6 +351,7 @@
             vmem((1, 1024), F32),
             vmem((64, 1024), BF16),
             vmem((1024, 1024), BF16),
+            vmem((512, 1024), BF16),
             vmem((512, 1024), BF16),
             vmem((1024, 1024), BF16),
             vmem((512, 512), BF16),
@@ -350,8 +372,8 @@
             pltpu.SemaphoreType.DMA((2,)),
             pltpu.SemaphoreType.DMA((2,)),
             *[pltpu.SemaphoreType.DMA((2, 2))] * 6,
-            pltpu.SemaphoreType.DMA((2,)),
-            pltpu.SemaphoreType.DMA((2,)),
+            pltpu.SemaphoreType.DMA((3,)),
+            pltpu.SemaphoreType.DMA((3,)),
         ],
         compiler_params=pltpu.CompilerParams(
             collective_id=0, has_side_effects=True, vmem_limit_bytes=60 << 20

time: 56.2 us -> 52.9 us (0.941)
  Pallas kernels: 55.1 us -> 51.9 us
    pallas_call x1, Pallas kernels: 55.1 us -> 51.9 us  [on_device(): pl.pallas_call(kernel, out_shape=vmem((2, 2048, 128), BF16), in_specs=[pl...]
where the time goes in v3:
time: 52.9 us
  Pallas kernels  51.9 us (98%)
  local copies, waits for them, and re-layouts  0.97 us (2%)
    pallas_call x1, Pallas kernels, on_device(): pl.pallas_call(kernel, out_shape=vmem((2, 2048, 128), BF16), in_specs=[pl...  51.9 us

profile of v3, /device:TPU:1, one launch (start us, length us, event | category | flops | bytes accessed | tf_op | source)
XLA Modules:
  0.0 52.9 jit_solution(10030719522303735916)
XLA Ops:
  0.0 51.9 %shard_map.100 = bf16[2,2048,128]{2,1,0:T(8,128)(2,1)S(1)} custom-call(bf16[2,2048,1024]{2,1,0:T(8,128)(2,1)} %tok.1, f32[1,1024]{1,0:T(1,128)} %bitcast.3, bf16[64,1024]{1,0:T(8,128)(2,1)} %bitcast.2, bf16[1024,1024]{1,0:T(8,128)(2,1)} %wgate.1, bf16[512,1024]{1,0:T(8,128)(2,1)} %wspec.1, bf16[1024,128]{1,0:T(8,128)(2,1)} %wout.1, ...), custom_call_target="tpu_custom_call" | custom-call | tf_op jit(solution)/shard_map/pallas_call | solution.py:344
  51.9 1.0 %copy.12 = bf16[2,2048,128]{2,1,0:T(8,128)(2,1)} copy(bf16[2,2048,128]{2,1,0:T(8,128)(2,1)S(1)} %shard_map.100) | data formatting | bytes 2097152
